TPU v7x, 32 devices: a whole 2x2x4 slice. The times are simulated.
32 devices in a mesh: ep: 16 (over z, y, x), tp: 2 (over core).
Axes of the slice: x: 2, y: 2, z: 4, core: 2. Of those that a mesh axis runs over, the one named last changes fastest.
Arguments:
- inputs: bfloat16 [256, 2048], P('ep'), may hold values from -6 to 6
- positions: int32 [256], P('ep'), may hold values from 1024 to 8191
- ret_state: float32 [256, 12, 128, 128], P('ep', 'tp'), may hold values from -4 to 4
- norm_mix: bfloat16 [2048], replicated, may hold values from 0.099609375 to 1.8984375
- w_query: bfloat16 [2048, 1536], P('ep', 'tp'), may hold values from -0.1875 to 0.1875
- w_key: bfloat16 [2048, 1536], P('ep', 'tp'), may hold values from -0.1875 to 0.1875
- w_value: bfloat16 [2048, 1536], P('ep', 'tp'), may hold values from -0.1875 to 0.1875
- w_gate_in: bfloat16 [2048, 1536], P('ep', 'tp'), may hold values from -0.1875 to 0.1875
- head_gain: bfloat16 [1536], P('tp'), may hold values from 0.099609375 to 1.8984375
- w_out: bfloat16 [1536, 2048], P('tp', 'ep'), may hold values from -0.15625 to 0.15625
- norm_ffn: bfloat16 [2048], replicated, may hold values from 0.099609375 to 1.8984375
- route_ids: int32 [256, 4], P('ep'), may hold values from 0 to 15, all different within a row; in each aligned block of 16 rows (0 to 15, 16 to 31, ...) at most 8 rows name the same one
- route_weight: bfloat16 [256, 4], P('ep'), may hold values from 0.19921875 to 1
- exp_gate: bfloat16 [16, 2048, 1024], P('ep', None, 'tp'), may hold values from -0.125 to 0.125
- exp_up: bfloat16 [16, 2048, 1024], P('ep', None, 'tp'), may hold values from -0.125 to 0.125
- exp_down: bfloat16 [16, 1024, 2048], P('ep', 'tp'), may hold values from -0.1875 to 0.1875
- dense_gate: bfloat16 [2048, 4096], P(None, ('ep', 'tp')), may hold values from -0.125 to 0.125
- dense_up: bfloat16 [2048, 4096], P(None, ('ep', 'tp')), may hold values from -0.125 to 0.125
- dense_down: bfloat16 [4096, 2048], P(('ep', 'tp')), may hold values from -0.1875 to 0.1875
- branch_gate: bfloat16 [2048], replicated, may hold values from -0.125 to 0.125
Outputs:
- layer_out: bfloat16 [256, 2048], P('ep')
- new_state: float32 [256, 12, 128, 128], P('ep', 'tp')
Inputs may be any that keep to these rules, and one draw needn't show every extreme that they name: `route_ids`: each row names 4 different experts. Among the rows of one index of ep no expert is named more than 8 times, a bound that some block reaches.
All inputs are finite; a program needn't handle non-finite values.
Results may differ from a plain program's by a relative error of at most 0.015.
Values may be sent and summed in bfloat16 or wider, within the bound.
A program may use at most 128 MiB of HBM per device.

v0:
```python
import jax
import jax.numpy as jnp
from jax import lax
from jax.sharding import PartitionSpec as P

D = 2048
HEADS = 12


EPS = 1e-06


def rms_scale(values, scales):
    widened = values.astype(jnp.float32)
    scaled = widened * lax.rsqrt(jnp.mean(widened * widened, axis=-1, keepdims=True) + EPS)
    return (scaled * scales.astype(jnp.float32)).astype(jnp.bfloat16)


def rotary_angles(positions, head_dim):
    halfway = head_dim // 2
    frequency = 10000.0 ** (-jnp.arange(halfway, dtype=jnp.float32) * 2.0 / head_dim)
    return positions.astype(jnp.float32)[:, None] * frequency[None, :]


def rotate_heads(values, angles):
    halfway = values.shape[-1] // 2
    cosine = jnp.cos(angles)[:, None, :]
    sine_of = jnp.sin(angles)[:, None, :]
    leading = values[..., :halfway]
    trailing = values[..., halfway:]
    return jnp.concatenate(
        [leading * cosine - trailing * sine_of, trailing * cosine + leading * sine_of], axis=-1
    )


def log_decay(head_count):
    spread = jnp.arange(head_count, dtype=jnp.float32) * (5.0 / max(head_count - 1, 1))
    return jnp.log1p(-(2.0 ** (-5.0 - spread)))


def retain(queries, keys_in, values_in, gate_pre, old_state, positions, scales, log_gamma):
    row_count, head_count, head_dim = (old_state.shape[0], old_state.shape[1], old_state.shape[2])
    angles = rotary_angles(positions, head_dim)
    rot_query = rotate_heads(
        queries.astype(jnp.float32).reshape(row_count, head_count, head_dim), angles
    )
    rot_key = rotate_heads(
        keys_in.astype(jnp.float32).reshape(row_count, head_count, head_dim), angles
    ) * head_dim ** (-0.5)
    value_heads = values_in.astype(jnp.float32).reshape(row_count, head_count, head_dim)
    new_state = (
        jnp.exp(log_gamma)[None, :, None, None] * old_state
        + rot_key[:, :, :, None] * value_heads[:, :, None, :]
    )
    readout = jnp.einsum("shd,shdv->shv", rot_query, new_state, precision=lax.Precision.HIGHEST)
    centred = readout - jnp.mean(readout, axis=-1, keepdims=True)
    normed = centred * lax.rsqrt(jnp.mean(centred * centred, axis=-1, keepdims=True) + EPS)
    normed = normed * scales.astype(jnp.float32).reshape(head_count, head_dim)
    gated_out = normed.reshape(row_count, head_count * head_dim) * jax.nn.silu(
        gate_pre.astype(jnp.float32)
    )
    return (gated_out.astype(jnp.bfloat16), new_state)


def slot_of(route_ids, expert_count, capacity):
    flat_ids = route_ids.reshape(-1)
    onehot = (flat_ids[:, None] == jnp.arange(expert_count, dtype=jnp.int32)[None, :]).astype(
        jnp.int32
    )
    ranking = jnp.sum((jnp.cumsum(onehot, axis=0) - 1) * onehot, axis=1)
    return flat_ids * capacity + ranking


def on_device(
    inputs,
    positions,
    ret_state,
    norm_mix,
    w_query,
    w_key,
    w_value,
    w_gate_in,
    head_gain,
    w_out,
    norm_ffn,
    route_ids,
    route_weight,
    exp_gate,
    exp_up,
    exp_down,
    dense_gate,
    dense_up,
    dense_down,
    branch_gate,
):
    seq_count = inputs.shape[0]
    top_count = route_ids.shape[1]
    ep_size = lax.axis_size("ep")
    local_experts = exp_gate.shape[0]
    expert_count = ep_size * local_experts
    capacity = max(2, 2 * seq_count * top_count // expert_count)
    normed = rms_scale(inputs, norm_mix)
    columns = lax.all_to_all(normed, "ep", split_axis=1, concat_axis=0, tiled=True)
    joined = jnp.concatenate([w_query, w_key, w_value, w_gate_in], axis=1)
    segment = columns
    summed = lax.psum_scatter(
        jnp.dot(segment, joined, preferred_element_type=jnp.float32),
        "ep",
        scatter_dimension=0,
        tiled=True,
    ).astype(jnp.bfloat16)
    queries, keys_new, values_new, gate_pre = jnp.split(summed, 4, axis=1)
    local_heads = ret_state.shape[1]
    log_gamma = lax.dynamic_slice_in_dim(
        log_decay(HEADS), lax.axis_index("tp") * local_heads, local_heads
    )
    retained, new_state = retain(
        queries, keys_new, values_new, gate_pre, ret_state, positions, head_gain, log_gamma
    )
    partial_cols = jnp.dot(
        lax.all_gather(retained, "ep", axis=0, tiled=True),
        w_out,
        preferred_element_type=jnp.float32,
    )
    rounded = lax.optimization_barrier(partial_cols.astype(jnp.bfloat16)).astype(jnp.float32)
    mixer_cols = lax.psum(rounded.astype(jnp.bfloat16), "tp")
    mixer_out = lax.all_to_all(mixer_cols, "ep", split_axis=0, concat_axis=1, tiled=True)
    residual_sum = (inputs.astype(jnp.float32) + mixer_out.astype(jnp.float32)).astype(jnp.bfloat16)
    normed_ffn = rms_scale(residual_sum, norm_ffn)
    slot_index = slot_of(route_ids, expert_count, capacity)
    slot_total = expert_count * capacity
    placing = (jnp.arange(slot_total, dtype=jnp.int32)[:, None] == slot_index[None, :]).astype(
        jnp.float32
    )
    by_token = jnp.sum(placing.reshape(slot_total, seq_count, top_count), axis=2)
    outgoing = (
        jnp.dot(by_token.astype(jnp.bfloat16), normed_ffn, preferred_element_type=jnp.float32)
        .astype(jnp.bfloat16)
        .reshape(expert_count, capacity, D)
    )
    received = lax.all_to_all(outgoing, "ep", split_axis=0, concat_axis=0, tiled=True)
    slot_count = received.shape[1]
    grouped = received.reshape(ep_size, local_experts, slot_count, D)
    gate_part = jnp.einsum("sjnd,jdf->sjnf", grouped, exp_gate, preferred_element_type=jnp.float32)
    up_part = jnp.einsum("sjnd,jdf->sjnf", grouped, exp_up, preferred_element_type=jnp.float32)
    hidden = (jax.nn.silu(gate_part) * up_part).astype(jnp.bfloat16)
    partial_out = jnp.einsum(
        "sjnf,jfd->sjnd", hidden, exp_down, preferred_element_type=jnp.float32
    ).reshape(received.shape[0], slot_count, D)
    returned = lax.all_to_all(
        partial_out.astype(jnp.bfloat16), "ep", split_axis=0, concat_axis=0, tiled=True
    ).astype(partial_out.dtype)
    widened = route_weight.astype(jnp.float32)
    share_flat = (widened / jnp.sum(widened, axis=-1, keepdims=True)).reshape(-1)
    weighting = jnp.sum(
        (placing * share_flat[None, :]).reshape(slot_total, seq_count, top_count), axis=2
    )
    expert_part = jnp.einsum(
        "rt,rd->td", weighting, returned.reshape(slot_total, D), precision=lax.Precision.HIGHEST
    )
    segment = lax.all_gather(normed_ffn, "ep", axis=0, tiled=True)
    gate_part = jnp.dot(segment, dense_gate, preferred_element_type=jnp.float32)
    up_part = jnp.dot(segment, dense_up, preferred_element_type=jnp.float32)
    hidden = (jax.nn.silu(gate_part) * up_part).astype(jnp.bfloat16)
    opening = jax.nn.sigmoid(
        jnp.dot(segment, branch_gate[:, None], preferred_element_type=jnp.float32)
    )
    branch_term = jnp.dot(hidden, dense_down, preferred_element_type=jnp.float32) * opening
    summed_branch = lax.psum_scatter(branch_term, "ep", scatter_dimension=0, tiled=True)
    summed_branch = summed_branch + expert_part
    width_total = lax.psum(summed_branch.astype(jnp.bfloat16), "tp").astype(jnp.float32)
    layer_out = (residual_sum.astype(jnp.float32) + width_total).astype(jnp.bfloat16)
    return (layer_out, new_state)


def solution(mesh):
    in_specs = (
        P("ep", None),
        P("ep"),
        P("ep", "tp", None, None),
        P(),
        P("ep", "tp"),
        P("ep", "tp"),
        P("ep", "tp"),
        P("ep", "tp"),
        P("tp"),
        P("tp", "ep"),
        P(),
        P("ep", None),
        P("ep", None),
        P("ep", None, "tp"),
        P("ep", None, "tp"),
        P("ep", "tp", None),
        P(None, ("ep", "tp")),
        P(None, ("ep", "tp")),
        P(("ep", "tp"), None),
        P(),
    )
    out_specs = (P("ep", None), P("ep", "tp", None, None))
    return jax.shard_map(
        on_device, mesh=mesh, in_specs=in_specs, out_specs=out_specs, check_vma=False
    )
```

profile of v0, /device:TPU:29, one launch (start us, length us, event | category | flops | bytes accessed | tf_op | source)
XLA Modules:
  0.0 407.8 jit_solution(14892159099410248619)
XLA Ops:
  7.2 0.8 convert_element_type.89
  8.1 1.0 fusion.39
  9.0 0.9 copy_bitcast_fusion
  10.0 9.5 %all_to_all.42 = bf16[16,16,128]{2,0,1:T(8,128)(2,1)S(1)} all-to-all(bf16[16,16,128]{2,0,1:T(8,128)(2,1)S(1)} %copy_bitcast_fusion), channel_id=1, replica_groups=mesh['ep'=16,'tp'=2] {'ep'}, dimensions={1} | all-to-all | bytes 131072 | tf_op jit(solution)/shard_map/all_to_all | solution.py:103
  19.4 3.4 fusion.25
  22.9 0.0 all-reduce.3.cloned.1.call-start
  22.9 0.6 copy-done.11
  23.5 0.1 dynamic-slice_exponential_fusion
  23.6 0.1 multiply_cosine_fusion
  23.8 130.0 %reduce-scatter.3.cloned.1.call-done = f32[16,3072]{1,0:T(8,128)} async-done(((f32[256,3072]{1,0:T(8,128)}), f32[16,3072]{1,0:T(8,128)}) %reduce-scatter.3.cloned.1.call-update) | async-done | bytes 196624 | tf_op jit(solution)/shard_map/reduce_scatter | solution.py:106
  153.8 0.9 convert_element_type.91
  154.8 0.1 multiply_subtract_fusion.1
  154.9 0.1 maximum_multiply_fusion
  155.0 0.1 maximum_bitcast_fusion
  155.1 4.5 %multiply_add_fusion = f32[16,6,128,128]{3,2,1,0:T(8,128)S(1)} fusion(f32[16,6,128,128]{3,2,1,0:T(8,128)} %param.22, f32[16,6,128]{2,1,0:T(8,128)S(1)} %reshape.211, f32[16,6,128]{2,1,0:T(8,128)S(1)} %maximum_multiply_fusion, f32[6]{0:T(128)S(1)} %dynamic-slice_exponential_fusion), kind=kLoop, calls=%fused_computation | loop fusion | flops 4718592 | bytes 12681240 | tf_op jit(solution)/shard_map/add | solution.py:52
  159.6 5.5 %fusion.63 = f32[16,6,1,128]{3,2,1,0:T(1,128)S(1)} fusion(f32[16,6,128,128]{3,2,1,0:T(8,128)S(1)} %multiply_add_fusion, f32[16,6,128,1]{2,1,0,3:T(8,128)S(1)} %maximum_bitcast_fusion), kind=kOutput, calls=%fused_computation.76 | convolution fusion | flops 18874368 | bytes 6389760 | tf_op jit(solution)/shard_map/shd,shdv->shv/dot_general | solution.py:55
  165.0 0.1 bitcast_reduce_fusion
  165.2 0.2 fusion.56
  165.3 0.1 fusion.57
  165.5 29.4 %all_gather.6 = bf16[256,768]{1,0:T(8,128)(2,1)S(1)} all-gather(bf16[16,768]{1,0:T(8,128)(2,1)S(1)} %fusion.65), channel_id=1, replica_groups=mesh['ep'=16,'tp'=2] {'ep'}, dimensions={0}, use_global_device_ids=true | all-gather | bytes 417792 | tf_op jit(solution)/shard_map/all_gather | solution.py:121
  194.8 0.9 convolution_convert_fusion.2
  195.8 28.7 %all-reduce.3.cloned.1.call-done = bf16[16,16,128]{2,1,0:T(8,128)(2,1)} async-done(((bf16[16,16,128]{2,1,0:T(8,128)(2,1)}), bf16[16,16,128]{2,1,0:T(8,128)(2,1)}) %all-reduce.3.cloned.1.call-update) | async-done | bytes 65552 | tf_op jit(solution)/shard_map/psum | solution.py:126
  224.5 6.4 %all-to-all-start.1 = ((bf16[16,16,128]{2,1,0:T(8,128)(2,1)}), bf16[16,16,128]{2,1,0:T(8,128)(2,1)S(1)}, u32[]{:S(2)}, u32[]{:S(2)}) async-start(bf16[16,16,128]{2,1,0:T(8,128)(2,1)} %all-reduce.3.cloned.1.call-done), calls=%async_computation.2 | async-start | bytes 131072 | tf_op jit(solution)/shard_map/all_to_all | solution.py:127
  230.9 3.2 all-to-all-done.1
  234.1 0.1 fusion.43
  234.3 0.7 fusion.45
  235.1 52.6 %all-gather.2.cloned.1.call-done = bf16[256,2048]{1,0:T(8,128)(2,1)} async-done(((bf16[16,2048]{1,0:T(8,128)(2,1)}), bf16[256,2048]{1,0:T(8,128)(2,1)}) %all-gather.2.cloned.1.call-update) | async-done | bytes 1048592 | tf_op jit(solution)/shard_map/all_gather | solution.py:161
  287.7 1.7 fusion.73
  289.4 1.8 fusion.72
  291.2 3.3 convolution_multiply_fusion
  294.6 0.6 copy-done.6
  295.2 0.1 copy.38
  295.3 0.1 eq.31
  295.4 0.1 fusion.66
  295.5 0.1 reduce_window_sum.11
  295.6 0.2 select_reduce_fusion.1
  295.8 0.1 reduce_sum.79
  295.8 0.1 copy.39
  296.0 0.1 convert_reduce_fusion
  296.1 0.3 fusion
  296.4 20.9 %all_to_all.43 = bf16[16,8,2048]{2,1,0:T(8,128)(2,1)S(1)} all-to-all(bf16[16,8,2048]{2,1,0:T(8,128)(2,1)S(1)} %fusion), channel_id=1, replica_groups=mesh['ep'=16,'tp'=2] {'ep'}, dimensions={0} | all-to-all | bytes 1048576 | tf_op jit(solution)/shard_map/all_to_all | solution.py:141
  317.3 2.0 fusion.7
  319.4 2.4 convolution_convert_fusion
  321.8 22.2 %all_to_all.44 = bf16[16,8,2048]{2,1,0:T(8,128)(2,1)S(1)} all-to-all(bf16[16,8,2048]{2,1,0:T(8,128)(2,1)S(1)} %convolution_convert_fusion), channel_id=1, replica_groups=mesh['ep'=16,'tp'=2] {'ep'}, dimensions={0} | all-to-all | bytes 1048576 | tf_op jit(solution)/shard_map/all_to_all | solution.py:150
  344.0 23.1 %reduce-scatter.5.cloned.1.call-done = f32[16,2048]{1,0:T(8,128)} async-done(((f32[256,2048]{1,0:T(8,128)}), f32[16,2048]{1,0:T(8,128)}) %reduce-scatter.5.cloned.1.call-update) | async-done | bytes 131088 | tf_op jit(solution)/shard_map/reduce_scatter | solution.py:169
  367.1 1.9 fusion.1
  369.0 30.8 %all-reduce.5.cloned.1.call-done = bf16[16,2048]{1,0:T(8,128)(2,1)} async-done(((bf16[16,2048]{1,0:T(8,128)(2,1)}), bf16[16,2048]{1,0:T(8,128)(2,1)}) %all-reduce.5.cloned.1.call-update) | async-done | bytes 65552 | tf_op jit(solution)/shard_map/psum | solution.py:171
  399.8 1.5 fusion.46
  (50 shorter events, 0.5 us)
Async XLA Ops:
  7.2 312.2 %copy-start = (bf16[1,512,2048]{2,1,0:T(8,128)(2,1)S(1)}, bf16[1,512,2048]{2,1,0:T(8,128)(2,1)}, u32[]{:S(2)}) copy-start(bf16[1,512,2048]{2,1,0:T(8,128)(2,1)} %param.35) | copy-start | bytes 6291460
  7.2 146.6 %reduce-scatter.3.cloned.1.call-start = ((), (), s32[]{:S(2)}) async-start(), calls=%async_computation.6 | async-start | bytes 3342336 | tf_op jit(solution)/shard_map/reduce_scatter | solution.py:106
  22.9 0.7 copy-start.11
  22.9 0.8 copy-start.9
  22.9 201.6 %all-reduce.3.cloned.1.call-start = ((), (), s32[]{:S(2)}) async-start(), calls=%async_computation.7 | async-start | bytes 131072 | tf_op jit(solution)/shard_map/psum | solution.py:126
  159.5 5.5 %copy-start.1 = (f32[16,6,128,128]{3,2,1,0:T(8,128)}, f32[16,6,128,128]{3,2,1,0:T(8,128)S(1)}, u32[]{:S(2)}) copy-start(f32[16,6,128,128]{3,2,1,0:T(8,128)S(1)} %multiply_add_fusion) | copy-start | bytes 18874372
  159.5 35.3 %copy-start.5 = (bf16[768,128]{1,0:T(8,128)(2,1)S(1)}, bf16[768,128]{1,0:T(8,128)(2,1)}, u32[]{:S(2)}) copy-start(bf16[768,128]{1,0:T(8,128)(2,1)} %param.29) | copy-start | bytes 589828
  159.5 71.3 %copy-start.7 = (bf16[2048]{0:T(1024)(128)(2,1)S(1)}, bf16[2048]{0:T(1024)(128)(2,1)}, u32[]{:S(2)}) copy-start(bf16[2048]{0:T(1024)(128)(2,1)} %param.30) | copy-start | bytes 12292
  159.6 74.5 %copy-start.3 = (bf16[16,2048]{1,0:T(8,128)(2,1)S(1)}, bf16[16,2048]{1,0:T(8,128)(2,1)}, u32[]{:S(2)}) copy-start(bf16[16,2048]{1,0:T(8,128)(2,1)} %param.20) | copy-start | bytes 196612
  165.0 70.0 %copy-start.8 = (bf16[2048]{0:T(1024)(128)(2,1)S(1)}, bf16[2048]{0:T(1024)(128)(2,1)}, u32[]{:S(2)}) copy-start(bf16[2048]{0:T(1024)(128)(2,1)} %param.39) | copy-start | bytes 12292
  224.5 9.6 %all-to-all-start.1 = ((bf16[16,16,128]{2,1,0:T(8,128)(2,1)}), bf16[16,16,128]{2,1,0:T(8,128)(2,1)S(1)}, u32[]{:S(2)}, u32[]{:S(2)}) async-start(bf16[16,16,128]{2,1,0:T(8,128)(2,1)} %all-reduce.3.cloned.1.call-done), calls=%async_computation.2 | async-start | bytes 131072 | tf_op jit(solution)/shard_map/all_to_all | solution.py:127
  230.8 56.9 %all-gather.2.cloned.1.call-start = ((), (), s32[]{:S(2)}) async-start(), calls=%async_computation.8 | async-start | bytes 1114112 | tf_op jit(solution)/shard_map/all_gather | solution.py:161
  235.0 132.1 %reduce-scatter.5.cloned.1.call-start = ((), (), s32[]{:S(2)}) async-start(), calls=%async_computation.9 | async-start | bytes 2228224 | tf_op jit(solution)/shard_map/reduce_scatter | solution.py:169
  287.7 3.5 copy-start.2
  294.6 0.7 copy-start.6
  294.6 1.4 copy-start.10
  294.6 1.5 copy-start.4
  294.6 105.2 %all-reduce.5.cloned.1.call-start = ((), (), s32[]{:S(2)}) async-start(), calls=%async_computation.10 | async-start | bytes 131072 | tf_op jit(solution)/shard_map/psum | solution.py:171
Sparse Core Ops, SparseCore 0:
  23.0 130.6 reduce-scatter.2
  195.9 28.5 all-reduce.2
  235.1 52.5 all-gather.1
  294.7 72.3 reduce-scatter.4
  369.8 29.9 all-reduce.4
where the time goes:
time: 410 us; the launch traced here: 408 us
  waiting for transfers between devices  269 us (66%)
  blocking collectives  81.9 us (20%)
  matrix products  23.2 us (6%)
  between operations  14.1 us (3%)
  other arithmetic  11.8 us (3%)
  starting transfers between devices  6.56 us (2%)
    reduce_scatter x1, waiting for transfers between devices, on_device(): lax.psum_scatter(jnp.dot(segment, joined, preferred_element_type=jnp.floa...  130 us
    all_gather x1, waiting for transfers between devices, on_device(): segment = lax.all_gather(normed_ffn, 'ep', axis=0, tiled=True)  52.6 us
    psum x1, waiting for transfers between devices, on_device(): lax.psum(summed_branch.astype(jnp.bfloat16), 'tp').astype(jnp.float32)  30.8 us
    all_gather x1, blocking collectives, on_device(): lax.all_gather(retained, 'ep', axis=0, tiled=True)  29.4 us
    psum x1, waiting for transfers between devices, on_device(): mixer_cols = lax.psum(rounded.astype(jnp.bfloat16), 'tp')  28.7 us
    reduce_scatter x1, waiting for transfers between devices, on_device(): lax.psum_scatter(branch_term, 'ep', scatter_dimension=0, tiled=True)  23.1 us
    all_to_all x1, blocking collectives, on_device(): lax.all_to_all(partial_out.astype(jnp.bfloat16), 'ep', split_axis=0, conc...  22.2 us
    all_to_all x1, blocking collectives, on_device(): lax.all_to_all(outgoing, 'ep', split_axis=0, concat_axis=0, tiled=True)  20.9 us
  transfers between devices with their start and end apart: 6, of which 6 were waited for; matrix products, arithmetic and copies ran while one was open for 1% of the time, Pallas kernels for 0%

commit v1 on v0

v1 whole, which is shorter than its diff:
```python
import functools

import jax
import jax.numpy as jnp
from jax import lax
from jax.experimental import pallas as pl
from jax.experimental.pallas import tpu as pltpu
from jax.sharding import PartitionSpec as P

HEADS = 12
EPS = 1e-06
MESH = pl.DeviceIdType.MESH
LANES = 128
F32 = jnp.float32
BF16 = jnp.bfloat16
VMEM_LIMIT = 60 * 1024 * 1024


def rotary_angles(positions, head_dim):
    halfway = head_dim // 2
    frequency = 10000.0 ** (-jnp.arange(halfway, dtype=jnp.float32) * 2.0 / head_dim)
    return positions.astype(jnp.float32)[:, None] * frequency[None, :]


def log_decay(head_count):
    spread = jnp.arange(head_count, dtype=jnp.float32) * (5.0 / max(head_count - 1, 1))
    return jnp.log1p(-(2.0 ** (-5.0 - spread)))


def normalize(values, gain):
    scaled = values * lax.rsqrt(jnp.mean(values * values, axis=-1, keepdims=True) + EPS)
    return (scaled * gain.astype(F32)).astype(BF16)


def greet(n, me, tp, partner=None):
    barrier = pltpu.get_barrier_semaphore()

    @pl.loop(1, n)
    def _(k):
        pl.semaphore_signal(
            barrier, inc=1, device_id=(lax.rem(me + k, n), tp), device_id_type=MESH
        )

    if partner is not None:
        pl.semaphore_signal(barrier, inc=1, device_id=(me, partner), device_id_type=MESH)
    pl.semaphore_wait(barrier, n - 1 + (partner is not None))


def to_peer(src, dst, send, recv, k, ep, tp):
    return pltpu.make_async_remote_copy(
        src_ref=src,
        dst_ref=dst,
        send_sem=send.at[k],
        recv_sem=recv.at[k],
        device_id=(ep, tp),
        device_id_type=MESH,
    )


def scatter_start(n, me, tp, src, dst, send, recv):
    @pl.loop(1, n)
    def _(k):
        peer = lax.rem(me + k, n)
        to_peer(src.at[peer], dst.at[me], send, recv, k, peer, tp).start()


def scatter_wait(n, me, tp, src, dst, send, recv):
    @pl.loop(1, n)
    def _(k):
        peer = lax.rem(me + k, n)
        came = lax.rem(me + n - k, n)
        copy = to_peer(src.at[peer], dst.at[came], send, recv, k, peer, tp)
        copy.wait_send()
        copy.wait_recv()


def project_kernel(
    n, x_ref, gain_ref, share_ref, wq, wk, wv, wg, out_ref, share_out,
    blocks, columns, parts, landed, shares, send, recv,
):
    me, tp = lax.axis_index("ep"), lax.axis_index("tp")
    seqs, width = x_ref.shape
    block = width // n
    normed = normalize(x_ref[...].astype(F32), gain_ref[...])
    for j in range(n):
        blocks[j] = normed[:, j * block : (j + 1) * block]
    greet(n, me, tp)
    sems = lambda i: (send.at[i], recv.at[i])
    scatter_start(n, me, tp, blocks, columns, *sems(0))
    scatter_start(n, me, tp, share_ref, shares, *sems(1))
    columns[me] = blocks[me]
    shares[me] = share_ref[me]
    scatter_wait(n, me, tp, blocks, columns, *sems(0))
    rows = columns[...].reshape(n * seqs, block)
    local = wq.shape[1]
    for i, w in enumerate((wq, wk, wv, wg)):
        part = jnp.dot(rows, w[...], preferred_element_type=F32).astype(BF16)
        parts[:, :, i * local : (i + 1) * local] = part.reshape(n, seqs, local)
    scatter_start(n, me, tp, parts, landed, *sems(2))
    landed[me] = parts[me]
    scatter_wait(n, me, tp, share_ref, shares, *sems(1))
    share_out[...] = shares[...]
    scatter_wait(n, me, tp, parts, landed, *sems(2))
    for i in range(4):
        cut = slice(i * local, (i + 1) * local)
        total = lax.fori_loop(
            0,
            n,
            lambda j, acc: acc + landed[j, :, cut].astype(F32),
            jnp.zeros((seqs, local), F32),
        )
        out_ref[:, cut] = total.astype(BF16)


def project(n, x, gain, share, weights):
    seqs, width = x.shape
    cols = sum(w.shape[1] for w in weights)
    vmem = pl.BlockSpec(memory_space=pltpu.VMEM)
    return pl.pallas_call(
        functools.partial(project_kernel, n),
        out_shape=(
            jax.ShapeDtypeStruct((seqs, cols), BF16),
            jax.ShapeDtypeStruct(share.shape, F32),
        ),
        in_specs=[vmem] * 7,
        out_specs=(vmem, vmem),
        scratch_shapes=[
            pltpu.VMEM((n, seqs, width // n), BF16),
            pltpu.VMEM((n, seqs, width // n), BF16),
            pltpu.VMEM((n, seqs, cols), BF16),
            pltpu.VMEM((n, seqs, cols), BF16),
            pltpu.VMEM(share.shape, F32),
            pltpu.SemaphoreType.DMA((3, n)),
            pltpu.SemaphoreType.DMA((3, n)),
        ],
        compiler_params=pltpu.CompilerParams(
            collective_id=0, has_side_effects=True, vmem_limit_bytes=VMEM_LIMIT
        ),
    )(x, gain, share, *weights)


def retain_kernel(
    gamma_ref, q_ref, k_ref, v_ref, g_ref, gain_ref, cos_ref, sin_ref, state_ref,
    new_ref, out_ref, readout,
):
    seqs, dim = q_ref.shape
    gamma = gamma_ref[pl.program_id(0)]
    cos, sin = cos_ref[...], sin_ref[...]

    def rotated(ref):
        val = ref[...].astype(F32)
        return val * cos + pltpu.roll(val, dim // 2, 1) * sin

    query = rotated(q_ref).T
    key = (rotated(k_ref) * dim ** (-0.5)).T
    value = v_ref[...].astype(F32)
    for s in range(seqs):
        new = gamma * state_ref[s, 0] + key[:, s : s + 1] * value[s : s + 1, :]
        new_ref[s, 0] = new
        readout[s : s + 1, :] = jnp.sum(new * query[:, s : s + 1], axis=0, keepdims=True)
    read = readout[...]
    centred = read - jnp.mean(read, axis=-1, keepdims=True)
    normed = centred * lax.rsqrt(jnp.mean(centred * centred, axis=-1, keepdims=True) + EPS)
    gate = g_ref[...].astype(F32)
    out_ref[...] = (
        normed * gain_ref[...].astype(F32) * (gate * jax.nn.sigmoid(gate))
    ).astype(BF16)


def retain(gamma, joined, gain, cos, sin, state):
    seqs, heads, dim = state.shape[:3]
    piece = lambda i: pl.BlockSpec((seqs, dim), lambda h, i=i: (0, i * heads + h))
    whole = pl.BlockSpec((seqs, dim), lambda h: (0, 0))
    held = pl.BlockSpec((seqs, 1, dim, dim), lambda h: (0, h, 0, 0))
    return pl.pallas_call(
        retain_kernel,
        grid=(heads,),
        out_shape=(
            jax.ShapeDtypeStruct(state.shape, F32),
            jax.ShapeDtypeStruct((seqs, heads * dim), BF16),
        ),
        in_specs=[
            pl.BlockSpec(memory_space=pltpu.SMEM),
            piece(0), piece(1), piece(2), piece(3),
            pl.BlockSpec((1, dim), lambda h: (0, h)),
            whole, whole, held,
        ],
        out_specs=(held, pl.BlockSpec((seqs, dim), lambda h: (0, h))),
        scratch_shapes=[pltpu.VMEM((seqs, dim), F32)],
        compiler_params=pltpu.CompilerParams(vmem_limit_bytes=VMEM_LIMIT),
    )(gamma, joined, joined, joined, joined, gain, cos, sin, state)


def mix_kernel(
    n, x_ref, ret_ref, wout_ref, gain_ref, share_ref, open_w, eg_hbm, eu_hbm, ed_hbm,
    dg_hbm, du_hbm, dd_hbm, out_ref,
    heads, cols, cols_in, cols_sum, mixed, mixed_row, half_out, gathered, eg, eu, ed, dg, du, dd,
    hidden, dense_hidden, opening, other, other_in, own, summed, landed, final, final_in,
    load, send, recv, pair_send, pair_recv, relay_send, relay_recv,
):
    me, tp = lax.axis_index("ep"), lax.axis_index("tp")
    mate = 1 - tp
    seqs, width = x_ref.shape
    block, half = width // n, width // 2
    tokens = n * seqs
    loads = [
        pltpu.make_async_copy(src, dst, load.at[i])
        for i, (src, dst) in enumerate(
            ((eg_hbm.at[0], eg), (eu_hbm.at[0], eu), (dg_hbm, dg), (du_hbm, du),
             (ed_hbm.at[0], ed), (dd_hbm, dd))
        )
    ]
    for copy in loads:
        copy.start()
    greet(n, me, tp, mate)
    sems = lambda i: (send.at[i], recv.at[i])
    pair = lambda src, dst, i: to_peer(src, dst, pair_send, pair_recv, i, me, mate)

    @pl.loop(1, n)
    def _(k):
        peer = lax.rem(me + k, n)
        to_peer(ret_ref, heads.at[me], *sems(0), k, peer, tp).start()

    heads[me] = ret_ref[...]

    @pl.loop(1, n)
    def _(k):
        came = lax.rem(me + n - k, n)
        copy = to_peer(ret_ref, heads.at[came], *sems(0), k, lax.rem(me + k, n), tp)
        copy.wait_send()
        copy.wait_recv()

    part = jnp.dot(
        heads[...].reshape(tokens, ret_ref.shape[1]), wout_ref[...], preferred_element_type=F32
    )
    cols[...] = part.astype(BF16).reshape(n, seqs, block)
    swap = pair(cols, cols_in, 0)
    swap.start()
    swap.wait()
    cols_sum[...] = (cols[...].astype(F32) + cols_in[...].astype(F32)).astype(BF16)
    scatter_start(n, me, tp, cols_sum, mixed, *sems(1))
    mixed[me] = cols_sum[me]
    scatter_wait(n, me, tp, cols_sum, mixed, *sems(1))
    for j in range(n):
        mixed_row[:, j * block : (j + 1) * block] = mixed[j].astype(F32)
    residual = (x_ref[...].astype(F32) + mixed_row[...]).astype(BF16)
    mixed_row[...] = residual.astype(F32)
    normed = normalize(residual.astype(F32), gain_ref[...])
    for c in range(2):
        half_out[c] = normed[:, c * half : (c + 1) * half]

    @pl.loop(1, n)
    def _(k):
        peer = lax.rem(me + k, n)
        to_peer(half_out.at[tp], gathered.at[tp, me], *sems(2), k, peer, tp).start()

    for c in range(2):
        gathered[c, me] = half_out[c]

    @pl.loop(1, n)
    def _(k):
        came = lax.rem(me + n - k, n)
        copy = to_peer(
            half_out.at[tp], gathered.at[tp, came], *sems(2), k, lax.rem(me + k, n), tp
        )
        copy.wait_send()
        copy.wait_recv()
        to_peer(
            gathered.at[tp, came], gathered.at[tp, came], relay_send, relay_recv, k, me, mate
        ).start()

    for copy in loads:
        copy.wait()

    @pl.loop(1, n)
    def _(k):
        came = lax.rem(me + n - k, n)
        relay = to_peer(
            gathered.at[tp, came], gathered.at[mate, came], relay_send, relay_recv, k, me, mate
        )
        relay.wait_send()
        relay.wait_recv()

    def features(w, at):
        left = gathered[0].reshape(tokens, half)
        right = gathered[1].reshape(tokens, half)
        return jnp.dot(left, w[:half, at], preferred_element_type=F32) + jnp.dot(
            right, w[half:, at], preferred_element_type=F32
        )

    tile = min(256, eg.shape[1])

    @pl.loop(0, eg.shape[1] // tile)
    def _(j):
        at = pl.ds(pl.multiple_of(j * tile, tile), tile)
        gate = features(eg, at)
        hidden[:, at] = (gate * jax.nn.sigmoid(gate) * features(eu, at)).astype(BF16)

    every = slice(None)
    gate = features(dg, every)
    dense_hidden[...] = (gate * jax.nn.sigmoid(gate) * features(du, every)).astype(BF16)
    opening[...] = jax.nn.sigmoid(features(open_w, every))

    def branch(at):
        expert = jnp.dot(hidden[...], ed[:, at], preferred_element_type=F32)
        dense = jnp.dot(dense_hidden[...], dd[:, at], preferred_element_type=F32)
        share = share_ref[...].reshape(tokens, LANES)[:, :1]
        return expert * share + dense * opening[:, :1]

    wide = min(256, half)

    @pl.loop(0, half // wide)
    def _(j):
        src = pl.ds(pl.multiple_of(mate * half + j * wide, wide), wide)
        at = pl.ds(pl.multiple_of(j * wide, wide), wide)
        other[:, at] = branch(src).astype(BF16)

    swap = pair(other, other_in, 1)
    swap.start()

    @pl.loop(0, half // wide)
    def _(j):
        src = pl.ds(pl.multiple_of(tp * half + j * wide, wide), wide)
        at = pl.ds(pl.multiple_of(j * wide, wide), wide)
        own[:, at] = branch(src)

    swap.wait()
    summed[...] = (own[...] + other_in[...].astype(F32)).astype(BF16).reshape(n, seqs, half)
    scatter_start(n, me, tp, summed, landed, *sems(3))
    landed[me] = summed[me]
    scatter_wait(n, me, tp, summed, landed, *sems(3))
    total = lax.fori_loop(
        0, n, lambda j, acc: acc + landed[j].astype(F32), jnp.zeros((seqs, half), F32)
    )
    mine = mixed_row[:, pl.ds(pl.multiple_of(tp * half, half), half)]
    final[...] = (mine + total).astype(BF16)
    swap = pair(final, final_in, 2)
    swap.start()
    out_ref[:, pl.ds(pl.multiple_of(tp * half, half), half)] = final[...]
    swap.wait()
    out_ref[:, pl.ds(pl.multiple_of(mate * half, half), half)] = final_in[...]


def mix(n, x, retained, w_out, gain, share, open_w, weights):
    seqs, width = x.shape
    block, half, tokens = width // n, width // 2, n * seqs
    eg, eu, ed, dg, du, dd = weights
    vmem = pl.BlockSpec(memory_space=pltpu.VMEM)
    hbm = pl.BlockSpec(memory_space=pl.ANY)
    return pl.pallas_call(
        functools.partial(mix_kernel, n),
        out_shape=jax.ShapeDtypeStruct((seqs, width), BF16),
        in_specs=[vmem] * 6 + [hbm] * 6,
        out_specs=vmem,
        scratch_shapes=[
            pltpu.VMEM((n,) + retained.shape, BF16),
            pltpu.VMEM((n, seqs, block), BF16),
            pltpu.VMEM((n, seqs, block), BF16),
            pltpu.VMEM((n, seqs, block), BF16),
            pltpu.VMEM((n, seqs, block), BF16),
            pltpu.VMEM((seqs, width), F32),
            pltpu.VMEM((2, seqs, half), BF16),
            pltpu.VMEM((2, n, seqs, half), BF16),
            pltpu.VMEM(eg.shape[1:], BF16),
            pltpu.VMEM(eu.shape[1:], BF16),
            pltpu.VMEM(ed.shape[1:], BF16),
            pltpu.VMEM(dg.shape, BF16),
            pltpu.VMEM(du.shape, BF16),
            pltpu.VMEM(dd.shape, BF16),
            pltpu.VMEM((tokens, eg.shape[2]), BF16),
            pltpu.VMEM((tokens, dg.shape[1]), BF16),
            pltpu.VMEM((tokens, LANES), F32),
            pltpu.VMEM((tokens, half), BF16),
            pltpu.VMEM((tokens, half), BF16),
            pltpu.VMEM((tokens, half), F32),
            pltpu.VMEM((n, seqs, half), BF16),
            pltpu.VMEM((n, seqs, half), BF16),
            pltpu.VMEM((seqs, half), BF16),
            pltpu.VMEM((seqs, half), BF16),
            pltpu.SemaphoreType.DMA((6,)),
            pltpu.SemaphoreType.DMA((4, n)),
            pltpu.SemaphoreType.DMA((4, n)),
            pltpu.SemaphoreType.DMA((3,)),
            pltpu.SemaphoreType.DMA((3,)),
            pltpu.SemaphoreType.DMA((n,)),
            pltpu.SemaphoreType.DMA((n,)),
        ],
        compiler_params=pltpu.CompilerParams(
            collective_id=1, has_side_effects=True, vmem_limit_bytes=VMEM_LIMIT
        ),
    )(x, retained, w_out, gain, share, open_w, *weights)


def on_device(
    inputs,
    positions,
    ret_state,
    norm_mix,
    w_query,
    w_key,
    w_value,
    w_gate_in,
    head_gain,
    w_out,
    norm_ffn,
    route_ids,
    route_weight,
    exp_gate,
    exp_up,
    exp_down,
    dense_gate,
    dense_up,
    dense_down,
    branch_gate,
):
    n = lax.axis_size("ep")
    seqs, width = inputs.shape
    local_heads, head_dim = ret_state.shape[1], ret_state.shape[2]
    assert exp_gate.shape[0] == 1

    widened = route_weight.astype(F32)
    share = widened / jnp.sum(widened, axis=-1, keepdims=True)
    match = route_ids[None, :, :] == jnp.arange(n, dtype=jnp.int32)[:, None, None]
    by_expert = jnp.sum(jnp.where(match, share[None], 0.0), axis=2)
    by_expert = jnp.broadcast_to(by_expert[:, :, None], (n, seqs, LANES))
    angles = rotary_angles(positions, head_dim)
    cos, sin = jnp.cos(angles), jnp.sin(angles)
    cos = jnp.concatenate([cos, cos], axis=1)
    sin = jnp.concatenate([-sin, sin], axis=1)
    gamma = jnp.exp(
        lax.dynamic_slice_in_dim(
            log_decay(HEADS), lax.axis_index("tp") * local_heads, local_heads
        )
    )
    open_w = jnp.broadcast_to(branch_gate[:, None], (width, LANES))

    joined, shares = project(
        n, inputs, norm_mix[None, :], by_expert, (w_query, w_key, w_value, w_gate_in)
    )
    new_state, retained = retain(gamma, joined, head_gain[None, :], cos, sin, ret_state)
    layer_out = mix(
        n, inputs, retained, w_out, norm_ffn[None, :], shares, open_w,
        (exp_gate, exp_up, exp_down, dense_gate, dense_up, dense_down),
    )
    return (layer_out, new_state)


def solution(mesh):
    in_specs = (
        P("ep", None),
        P("ep"),
        P("ep", "tp", None, None),
        P(),
        P("ep", "tp"),
        P("ep", "tp"),
        P("ep", "tp"),
        P("ep", "tp"),
        P("tp"),
        P("tp", "ep"),
        P(),
        P("ep", None),
        P("ep", None),
        P("ep", None, "tp"),
        P("ep", None, "tp"),
        P("ep", "tp", None),
        P(None, ("ep", "tp")),
        P(None, ("ep", "tp")),
        P(("ep", "tp"), None),
        P(),
    )
    out_specs = (P("ep", None), P("ep", "tp", None, None))
    return jax.shard_map(
        on_device, mesh=mesh, in_specs=in_specs, out_specs=out_specs, check_vma=False
    )
```

time: 410 us -> 126 us (0.31)
  waiting for transfers between devices: 269 us -> 0 us
  Pallas kernels: 0 us -> 114 us
  blocking collectives: 81.9 us -> 0 us
  matrix products: 23.2 us -> 0 us
  between operations: 14.1 us -> 0.67 us
  other arithmetic: 11.8 us -> 3.57 us
  starting transfers between devices: 6.56 us -> 0 us
  local copies, waits for them, and re-layouts: 1.69 us -> 7.18 us
    reduce_scatter x2 -> x0, waiting for transfers between devices: 153 us -> none  [the longest x1 130 us: on_device(): lax.psum_scatter(jnp.dot(segment, joined, preferred_element_type=jnp.floa...]
    pallas_call x0 -> x3, Pallas kernels: none -> 114 us  [the longest x1 60.4 us: mix(): pl.pallas_call(functools.partial(mix_kernel, n), out_shape=jax.ShapeDtype...]
    psum x2 -> x0, waiting for transfers between devices: 59.5 us -> none  [the longest x1 30.8 us: on_device(): lax.psum(summed_branch.astype(jnp.bfloat16), 'tp').astype(jnp.float32)]
    all_gather x1 -> x0, waiting for transfers between devices: 52.6 us -> none  [on_device(): segment = lax.all_gather(normed_ffn, 'ep', axis=0, tiled=True)]
    all_to_all x3 -> x0, blocking collectives: 52.6 us -> none  [the longest x1 22.2 us: on_device(): lax.all_to_all(partial_out.astype(jnp.bfloat16), 'ep', split_axis=0, conc...]
    all_gather x1 -> x0, blocking collectives: 29.4 us -> none  [on_device(): lax.all_gather(retained, 'ep', axis=0, tiled=True)]
    dot_general x10 -> x0, matrix products: 23.2 us -> none  [the longest x1 5.46 us: retain(): jnp.einsum('shd,shdv->shv', rot_query, new_state, precision=lax.Precision...]
    all_to_all x1 -> x0, starting transfers between devices: 6.36 us -> none  [on_device(): lax.all_to_all(mixer_cols, 'ep', split_axis=0, concat_axis=1, tiled=True)]
  transfers between devices with their start and end apart: 6 -> 0, of which waited for: 6 -> 0; matrix products, arithmetic and copies ran while one was open for 1% -> 0% of each run, Pallas kernels for 0% -> 0%
where the time goes in v1:
time: 126 us
  Pallas kernels  114 us (90%)
  local copies, waits for them, and re-layouts  7.18 us (6%)
  other arithmetic  3.57 us (3%)
    pallas_call x1, Pallas kernels, mix(): pl.pallas_call(functools.partial(mix_kernel, n), out_shape=jax.ShapeDtype...  60.4 us
    pallas_call x1, Pallas kernels, project(): pl.pallas_call(functools.partial(project_kernel, n), out_shape=(jax.Shape...  44.1 us
    pallas_call x1, Pallas kernels, retain(): pl.pallas_call(retain_kernel, grid=(heads,), out_shape=(jax.ShapeDtypeStr...  9.68 us

profile of v1, /device:TPU:29, one launch (start us, length us, event | category | flops | bytes accessed | tf_op | source)
XLA Modules:
  0.0 125.6 jit_solution(12951866958088210905)
XLA Ops:
  0.6 0.7 convert_element_type.7
  1.3 0.1 fusion
  1.4 0.7 pad_maximum_fusion
  2.1 0.7 dynamic-slice_exponential_fusion.gamma_ref
  2.8 0.7 convert_reduce_fusion
  3.5 0.7 convert_divide_fusion
  4.2 0.7 select_reduce_fusion
  4.9 0.8 broadcast_in_dim.42.share_ref
  5.6 1.3 %broadcast_in_dim.22.gain_ref = bf16[1,2048]{1,0:T(2,128)(2,1)} reshape(bf16[2048]{0:T(1024)(128)(2,1)} %param.23) | data formatting | bytes 8192 | tf_op jit(solution)/shard_map/broadcast_in_dim | solution.py:438
  6.9 44.1 %shard_map.203 = (bf16[16,3072]{1,0:T(8,128)(2,1)}, f32[16,16,128]{2,1,0:T(8,128)}) custom-call(bf16[16,2048]{1,0:T(8,128)(2,1)} %x_ref.3, bf16[1,2048]{1,0:T(2,128)(2,1)} %broadcast_in_dim.22.gain_ref, f32[16,16,128]{2,1,0:T(8,128)} %broadcast_in_dim.42.share_ref, bf16[128,768]{1,0:T(8,128)(2,1)} %wq.1, bf16[128,768]{1,0:T(8,128)(2,1)} %wk.1, ...), custom_call_target="tpu_custom_call" | custom-call | tf_op jit(solution)/shard_map/pallas_call | solution.py:119
  51.0 1.3 %broadcast_in_dim.43.gain_ref = bf16[1,768]{1,0:T(2,128)(2,1)} reshape(bf16[768]{0:T(1024)(128)(2,1)} %param.28) | data formatting | bytes 3072 | tf_op jit(solution)/shard_map/broadcast_in_dim | solution.py:440
  52.3 0.0 copy-start
  52.3 0.0 copy-start.1
  52.3 9.7 %shard_map.204 = (f32[16,6,128,128]{3,2,1,0:T(8,128)}, bf16[16,768]{1,0:T(8,128)(2,1)}) custom-call(f32[6]{0:T(128)} %dynamic-slice_exponential_fusion.gamma_ref, bf16[16,3072]{1,0:T(8,128)(2,1)} %get-tuple-element.6.q_ref.k_ref.v_ref.g_ref, bf16[16,3072]{1,0:T(8,128)(2,1)} %get-tuple-element.6.q_ref.k_ref.v_ref.g_ref, ...), custom_call_target="tpu_custom_call" | custom-call | tf_op jit(solution)/shard_map/pallas_call | solution.py:175
  62.0 0.0 copy-done
  62.0 1.1 broadcast_in_dim.45.open_w
  63.1 0.0 copy-done.1
  63.1 0.6 broadcast_in_dim.44.gain_ref
  63.7 60.4 %shard_map.205 = bf16[16,2048]{1,0:T(8,128)(2,1)} custom-call(bf16[16,2048]{1,0:T(8,128)(2,1)} %x_ref.3, bf16[16,768]{1,0:T(8,128)(2,1)} %get-tuple-element.7.ret_ref, bf16[768,128]{1,0:T(8,128)(2,1)} %wout_ref.1, bf16[1,2048]{1,0:T(2,128)(2,1)} %broadcast_in_dim.44.gain_ref, f32[16,16,128]{2,1,0:T(8,128)} %get-tuple-element.8.share_ref, ...), custom_call_target="tpu_custom_call" | custom-call | tf_op jit(solution)/shard_map/pallas_call | solution.py:350
  124.2 1.5 %copy.25 = bf16[16,2048]{1,0:T(8,128)(2,1)} copy(bf16[16,2048]{1,0:T(8,128)(2,1)} %shard_map.205) | data formatting | bytes 131072
  (2 shorter events, 0.0 us)
Async XLA Ops:
  52.3 9.7 %copy-start = (bf16[2048]{0:T(1024)(128)(2,1)S(1)}, bf16[2048]{0:T(1024)(128)(2,1)}, u32[]{:S(2)}) copy-start(bf16[2048]{0:T(1024)(128)(2,1)} %param.39) | copy-start | bytes 12292
  52.3 10.8 %copy-start.1 = (bf16[2048]{0:T(1024)(128)(2,1)S(1)}, bf16[2048]{0:T(1024)(128)(2,1)}, u32[]{:S(2)}) copy-start(bf16[2048]{0:T(1024)(128)(2,1)} %param.30) | copy-start | bytes 12292

commit v2 on v1

--- a/solution.py
+++ b/solution.py
@@ -75,68 +75,135 @@
 
 
 def project_kernel(
-    n, x_ref, gain_ref, share_ref, wq, wk, wv, wg, out_ref, share_out,
-    blocks, columns, parts, landed, shares, send, recv,
+    n, x_ref, gain_ref, ids_ref, weight_ref, wq, wk, wv, wg, out_ref, share_out,
+    blocks, columns, parts, plane, reduced, landed, share_ref, shares,
+    send, recv, plane_send, plane_recv, line_send, line_recv,
 ):
     me, tp = lax.axis_index("ep"), lax.axis_index("tp")
     seqs, width = x_ref.shape
-    block = width // n
+    block, local = width // n, wq.shape[1]
+    outer, inner = parts.shape[2], parts.shape[1]
+    along, inside = me // inner, lax.rem(me, inner)
     normed = normalize(x_ref[...].astype(F32), gain_ref[...])
     for j in range(n):
         blocks[j] = normed[:, j * block : (j + 1) * block]
     greet(n, me, tp)
     sems = lambda i: (send.at[i], recv.at[i])
     scatter_start(n, me, tp, blocks, columns, *sems(0))
+    columns[me] = blocks[me]
+    widened = weight_ref[...].astype(F32)
+    part = widened / jnp.sum(widened, axis=-1, keepdims=True)
+    for j in range(n):
+        mine = jnp.sum(jnp.where(ids_ref[...] == j, part, 0.0), axis=-1, keepdims=True)
+        share_ref[j] = jnp.broadcast_to(mine, (seqs, LANES))
     scatter_start(n, me, tp, share_ref, shares, *sems(1))
-    columns[me] = blocks[me]
     shares[me] = share_ref[me]
     scatter_wait(n, me, tp, blocks, columns, *sems(0))
     rows = columns[...].reshape(n * seqs, block)
-    local = wq.shape[1]
+
+    def in_plane(i, k, source):
+        peer = lax.rem(inside + k, inner)
+        return to_peer(
+            parts.at[i, peer], plane.at[i, source], plane_send.at[i], plane_recv.at[i], k,
+            me - inside + peer, tp,
+        )
+
+    def in_line(i, k, source):
+        peer = lax.rem(along + k, outer)
+        return to_peer(
+            reduced.at[i, peer], landed.at[i, source], line_send.at[i], line_recv.at[i], k,
+            peer * inner + inside, tp,
+        )
+
+    span = inner * seqs
     for i, w in enumerate((wq, wk, wv, wg)):
-        part = jnp.dot(rows, w[...], preferred_element_type=F32).astype(BF16)
-        parts[:, :, i * local : (i + 1) * local] = part.reshape(n, seqs, local)
-    scatter_start(n, me, tp, parts, landed, *sems(2))
-    landed[me] = parts[me]
+        product = jnp.dot(rows, w[...], preferred_element_type=F32).astype(BF16)
+        for z in range(outer):
+            parts[i, :, z] = product[z * span : (z + 1) * span].reshape(inner, seqs, local)
+
+        @pl.loop(1, inner)
+        def _(k):
+            in_plane(i, k, inside).start()
+
+        plane[i, inside] = parts[i, inside]
+
+    for i in range(4):
+
+        @pl.loop(1, inner)
+        def _(k):
+            copy = in_plane(i, k, lax.rem(inside + inner - k, inner))
+            copy.wait_send()
+            copy.wait_recv()
+
+        for z in range(outer):
+            total = lax.fori_loop(
+                0,
+                inner,
+                lambda j, acc: acc + plane[i, j, z].astype(F32),
+                jnp.zeros((seqs, local), F32),
+            )
+            reduced[i, z] = total.astype(BF16)
+
+        @pl.loop(1, outer)
+        def _(k):
+            in_line(i, k, along).start()
+
+        landed[i, along] = reduced[i, along]
+
     scatter_wait(n, me, tp, share_ref, shares, *sems(1))
     share_out[...] = shares[...]
-    scatter_wait(n, me, tp, parts, landed, *sems(2))
     for i in range(4):
-        cut = slice(i * local, (i + 1) * local)
+
+        @pl.loop(1, outer)
+        def _(k):
+            copy = in_line(i, k, lax.rem(along + outer - k, outer))
+            copy.wait_send()
+            copy.wait_recv()
+
         total = lax.fori_loop(
             0,
-            n,
-            lambda j, acc: acc + landed[j, :, cut].astype(F32),
+            outer,
+            lambda j, acc: acc + landed[i, j].astype(F32),
             jnp.zeros((seqs, local), F32),
         )
-        out_ref[:, cut] = total.astype(BF16)
-
-
-def project(n, x, gain, share, weights):
+        out_ref[:, i * local : (i + 1) * local] = total.astype(BF16)
+
+
+def project(n, x, gain, ids, weight, weights):
     seqs, width = x.shape
-    cols = sum(w.shape[1] for w in weights)
+    local = weights[0].shape[1]
+    outer = 4 if n % 4 == 0 else 1
+    inner = n // outer
     vmem = pl.BlockSpec(memory_space=pltpu.VMEM)
+    sem = pltpu.SemaphoreType.DMA
     return pl.pallas_call(
         functools.partial(project_kernel, n),
         out_shape=(
-            jax.ShapeDtypeStruct((seqs, cols), BF16),
-            jax.ShapeDtypeStruct(share.shape, F32),
+            jax.ShapeDtypeStruct((seqs, 4 * local), BF16),
+            jax.ShapeDtypeStruct((n, seqs, LANES), F32),
         ),
-        in_specs=[vmem] * 7,
+        in_specs=[vmem] * 8,
         out_specs=(vmem, vmem),
         scratch_shapes=[
             pltpu.VMEM((n, seqs, width // n), BF16),
             pltpu.VMEM((n, seqs, width // n), BF16),
-            pltpu.VMEM((n, seqs, cols), BF16),
-            pltpu.VMEM((n, seqs, cols), BF16),
-            pltpu.VMEM(share.shape, F32),
-            pltpu.SemaphoreType.DMA((3, n)),
-            pltpu.SemaphoreType.DMA((3, n)),
+            pltpu.VMEM((4, inner, outer, seqs, local), BF16),
+            pltpu.VMEM((4, inner, outer, seqs, local), BF16),
+            pltpu.VMEM((4, outer, seqs, local), BF16),
+            pltpu.VMEM((4, outer, seqs, local), BF16),
+            pltpu.VMEM((n, seqs, LANES), F32),
+            pltpu.VMEM((n, seqs, LANES), F32),
+            sem((2, n)),
+            sem((2, n)),
+            sem((4, inner)),
+            sem((4, inner)),
+            sem((4, outer)),
+            sem((4, outer)),
         ],
         compiler_params=pltpu.CompilerParams(
             collective_id=0, has_side_effects=True, vmem_limit_bytes=VMEM_LIMIT
         ),
-    )(x, gain, share, *weights)
+    )(x, gain, ids, weight, *weights)
 
 
 def retain_kernel(
@@ -418,11 +485,6 @@
     local_heads, head_dim = ret_state.shape[1], ret_state.shape[2]
     assert exp_gate.shape[0] == 1
 
-    widened = route_weight.astype(F32)
-    share = widened / jnp.sum(widened, axis=-1, keepdims=True)
-    match = route_ids[None, :, :] == jnp.arange(n, dtype=jnp.int32)[:, None, None]
-    by_expert = jnp.sum(jnp.where(match, share[None], 0.0), axis=2)
-    by_expert = jnp.broadcast_to(by_expert[:, :, None], (n, seqs, LANES))
     angles = rotary_angles(positions, head_dim)
     cos, sin = jnp.cos(angles), jnp.sin(angles)
     cos = jnp.concatenate([cos, cos], axis=1)
@@ -435,7 +497,8 @@
     open_w = jnp.broadcast_to(branch_gate[:, None], (width, LANES))
 
     joined, shares = project(
-        n, inputs, norm_mix[None, :], by_expert, (w_query, w_key, w_value, w_gate_in)
+        n, inputs, norm_mix[None, :], route_ids, route_weight,
+        (w_query, w_key, w_value, w_gate_in),
     )
     new_state, retained = retain(gamma, joined, head_gain[None, :], cos, sin, ret_state)
     layer_out = mix(

time: 126 us -> 111 us (0.88)
  Pallas kernels: 114 us -> 98.8 us
  other arithmetic: 3.57 us -> 1.48 us
  local copies, waits for them, and re-layouts: 7.18 us -> 9.11 us
    pallas_call x1, Pallas kernels: 44.1 us -> 31.8 us  [project(): pl.pallas_call(functools.partial(project_kernel, n), out_shape=(jax.Shape...]
    pallas_call x1, Pallas kernels: 60.4 us -> 57.3 us  [mix(): pl.pallas_call(functools.partial(mix_kernel, n), out_shape=jax.ShapeDtype...]
    unnamed x5 -> x7, local copies, waits for them, and re-layouts: 1.48 us -> 4.18 us
    reduce_sum x2 -> x0, other arithmetic: 1.39 us -> none  [the longest x1 0.7 us: on_device(): by_expert = jnp.sum(jnp.where(match, share[None], 0.0), axis=2)]
where the time goes in v2:
time: 111 us; the launch traced here: 110 us
  Pallas kernels  98.8 us (89%)
  local copies, waits for them, and re-layouts  9.11 us (8%)
  other arithmetic  1.48 us (1%)
    pallas_call x1, Pallas kernels, mix(): pl.pallas_call(functools.partial(mix_kernel, n), out_shape=jax.ShapeDtype...  57.3 us
    pallas_call x1, Pallas kernels, project(): pl.pallas_call(functools.partial(project_kernel, n), out_shape=(jax.Shape...  31.8 us
    pallas_call x1, Pallas kernels, retain(): pl.pallas_call(retain_kernel, grid=(heads,), out_shape=(jax.ShapeDtypeStr...  9.68 us
    unnamed x7, local copies, waits for them, and re-layouts  4.18 us

profile of v2, /device:TPU:29, one launch (start us, length us, event | category | flops | bytes accessed | tf_op | source)
XLA Modules:
  0.0 110.0 jit_solution(5599057626274961713)
XLA Ops:
  0.6 0.7 convert_element_type.3
  1.3 0.1 fusion
  1.4 0.7 pad_maximum_fusion
  2.1 0.6 dynamic-slice_exponential_fusion.gamma_ref
  2.8 1.3 %broadcast_in_dim.8.gain_ref = bf16[1,2048]{1,0:T(2,128)(2,1)} reshape(bf16[2048]{0:T(1024)(128)(2,1)} %param.23) | data formatting | bytes 8192 | tf_op jit(solution)/shard_map/broadcast_in_dim | solution.py:500
  4.0 1.4 %copy.22.ids_ref = s32[16,4]{1,0:T(8,128)} copy(s32[16,4]{0,1:T(4,128)} %param.31) | data formatting | bytes 512 | tf_op args[11]
  5.4 1.3 %copy.23.weight_ref = bf16[16,4]{1,0:T(8,128)(2,1)} copy(bf16[16,4]{0,1:T(4,128)(2,1)} %param.32) | data formatting | bytes 256 | tf_op args[12]
  6.7 31.8 %shard_map.203 = (bf16[16,3072]{1,0:T(8,128)(2,1)}, f32[16,16,128]{2,1,0:T(8,128)}) custom-call(bf16[16,2048]{1,0:T(8,128)(2,1)} %x_ref.3, bf16[1,2048]{1,0:T(2,128)(2,1)} %broadcast_in_dim.8.gain_ref, s32[16,4]{1,0:T(8,128)} %copy.22.ids_ref, bf16[16,4]{1,0:T(8,128)(2,1)} %copy.23.weight_ref, bf16[128,768]{1,0:T(8,128)(2,1)} %wq.1, bf16[128,768]{1,0:T(8,128)(2,1)} %wk.1, ...), custom_call_target="tpu_custom_call" | custom-call | tf_op jit(solution)/shard_map/pallas_call | solution.py:179
  38.6 1.3 %broadcast_in_dim.18.gain_ref = bf16[1,768]{1,0:T(2,128)(2,1)} reshape(bf16[768]{0:T(1024)(128)(2,1)} %param.28) | data formatting | bytes 3072 | tf_op jit(solution)/shard_map/broadcast_in_dim | solution.py:503
  39.8 0.0 copy-start
  39.8 0.0 copy-start.1
  39.8 9.7 %shard_map.204 = (f32[16,6,128,128]{3,2,1,0:T(8,128)}, bf16[16,768]{1,0:T(8,128)(2,1)}) custom-call(f32[6]{0:T(128)} %dynamic-slice_exponential_fusion.gamma_ref, bf16[16,3072]{1,0:T(8,128)(2,1)} %get-tuple-element.6.q_ref.k_ref.v_ref.g_ref, bf16[16,3072]{1,0:T(8,128)(2,1)} %get-tuple-element.6.q_ref.k_ref.v_ref.g_ref, ...), custom_call_target="tpu_custom_call" | custom-call | tf_op jit(solution)/shard_map/pallas_call | solution.py:242
  49.5 0.0 copy-done
  49.5 1.1 %broadcast_in_dim.20.open_w = bf16[2048,128]{1,0:T(8,128)(2,1)} broadcast(bf16[2048]{0:T(1024)(128)(2,1)S(1)} %copy-done), dimensions={0} | broadcast | bytes 528384 | tf_op jit(solution)/shard_map/broadcast_in_dim | solution.py:497
  50.7 0.0 copy-done.1
  50.7 0.6 broadcast_in_dim.19.gain_ref
  51.3 57.3 %shard_map.205 = bf16[16,2048]{1,0:T(8,128)(2,1)} custom-call(bf16[16,2048]{1,0:T(8,128)(2,1)} %x_ref.3, bf16[16,768]{1,0:T(8,128)(2,1)} %get-tuple-element.7.ret_ref, bf16[768,128]{1,0:T(8,128)(2,1)} %wout_ref.1, bf16[1,2048]{1,0:T(2,128)(2,1)} %broadcast_in_dim.19.gain_ref, f32[16,16,128]{2,1,0:T(8,128)} %get-tuple-element.8.share_ref, ...), custom_call_target="tpu_custom_call" | custom-call | tf_op jit(solution)/shard_map/pallas_call | solution.py:417
  108.6 1.5 %copy.25 = bf16[16,2048]{1,0:T(8,128)(2,1)} copy(bf16[16,2048]{1,0:T(8,128)(2,1)} %shard_map.205) | data formatting | bytes 131072
  (2 shorter events, 0.0 us)
Async XLA Ops:
  39.8 9.7 %copy-start = (bf16[2048]{0:T(1024)(128)(2,1)S(1)}, bf16[2048]{0:T(1024)(128)(2,1)}, u32[]{:S(2)}) copy-start(bf16[2048]{0:T(1024)(128)(2,1)} %param.39) | copy-start | bytes 12292
  39.8 10.8 %copy-start.1 = (bf16[2048]{0:T(1024)(128)(2,1)S(1)}, bf16[2048]{0:T(1024)(128)(2,1)}, u32[]{:S(2)}) copy-start(bf16[2048]{0:T(1024)(128)(2,1)} %param.30) | copy-start | bytes 12292
